TPU v7x, 32 devices: a whole 2x2x4 slice. The times are simulated.
32 devices in a mesh: kv: 8 (over z, y), tp: 4 (over x, core).
Axes of the slice: x: 2, y: 2, z: 4, core: 2. Of those that a mesh axis runs over, the one named last changes fastest.
Arguments:
- tokens: bfloat16 [128, 4096], P('tp', 'kv')
- seq_pos: int32 [128], P('kv'), may hold values from 0 to 4095
- state: float32 [128, 16, 128, 256], P('kv', 'tp'), may hold values from -0.6 to 0.6
- norm_in_gain: float32 [4096], P('kv'), may hold values from 0.1 to 1.9
- query_weight: bfloat16 [4096, 2048], P('kv', 'tp'), may hold values from -0.09375 to 0.09375
- key_weight: bfloat16 [4096, 2048], P('kv', 'tp'), may hold values from -0.09375 to 0.09375
- value_weight: bfloat16 [4096, 4096], P('kv', 'tp'), may hold values from -0.09375 to 0.09375
- gate_weight: bfloat16 [4096, 4096], P('kv', 'tp'), may hold values from -0.09375 to 0.09375
- head_gain: float32 [4096], P('tp'), may hold values from 0.1 to 1.9
- out_weight: bfloat16 [4096, 4096], P('tp', 'kv'), may hold values from -0.09375 to 0.09375
- norm_mlp_gain: float32 [4096], P('kv'), may hold values from 0.1 to 1.9
- hidden_weight: bfloat16 [4096, 16384], P('kv', 'tp'), may hold values from -0.09375 to 0.09375
- down_weight: bfloat16 [16384, 4096], P('tp', 'kv'), may hold values from -0.046875 to 0.046875
Outputs:
- output: bfloat16 [128, 4096], P('tp', 'kv')
- new_state: float32 [128, 16, 128, 256], P('kv', 'tp')
All inputs are finite; a program needn't handle non-finite values.
Results may differ from a plain program's by a relative error of at most 0.03.
Values may be sent and summed in bfloat16 or wider, within the bound.
A program may use at most 64 MiB of HBM per device.

v0:
```python
import jax
import jax.numpy as jnp
from jax import lax
from jax.sharding import PartitionSpec as P

D = 4096
H = 16
DK = 128
DV = 256
EPS = 1e-06


def rotate(vectors, positions):
    half = vectors.shape[-1] // 2
    inverse = jnp.power(10000.0, -jnp.arange(half, dtype=jnp.float32) / half)
    angles = positions.astype(jnp.float32)[:, None] * inverse[None, :]
    cosine = jnp.cos(angles)[:, None, :]
    sine = jnp.sin(angles)[:, None, :]
    first, second = (vectors[..., :half], vectors[..., half:])
    return jnp.concatenate(
        [first * cosine - second * sine, first * sine + second * cosine], axis=-1
    )


def head_decay(head_ids):
    return 1.0 - jnp.exp2(-2.0 - 6.0 * head_ids / (H - 1))


def local(
    tokens,
    seq_pos,
    state,
    norm_in_gain,
    query_weight,
    key_weight,
    value_weight,
    gate_weight,
    head_gain,
    out_weight,
    norm_mlp_gain,
    hidden_weight,
    down_weight,
):
    rows_all = lax.all_gather(tokens, "tp", axis=0, tiled=True)
    rows_f = rows_all.astype(jnp.float32)
    squares_in = jnp.sum(rows_f * rows_f, axis=1)
    normed_in = (rows_f * norm_in_gain[None, :]).astype(jnp.bfloat16)
    term_query = jnp.dot(normed_in, query_weight, preferred_element_type=jnp.float32).astype(
        jnp.bfloat16
    )
    term_keys = jnp.dot(normed_in, key_weight, preferred_element_type=jnp.float32).astype(
        jnp.bfloat16
    )
    term_values = jnp.dot(normed_in, value_weight, preferred_element_type=jnp.float32).astype(
        jnp.bfloat16
    )
    term_gates = jnp.dot(normed_in, gate_weight, preferred_element_type=jnp.float32).astype(
        jnp.bfloat16
    )
    total_all = lax.psum(squares_in, "kv")
    query, keys, values, gates = (
        lax.psum_scatter(term_query, "kv", scatter_dimension=0, tiled=True).astype(jnp.float32),
        lax.psum_scatter(term_keys, "kv", scatter_dimension=0, tiled=True).astype(jnp.float32),
        lax.psum_scatter(term_values, "kv", scatter_dimension=0, tiled=True).astype(jnp.float32),
        lax.psum_scatter(term_gates, "kv", scatter_dimension=0, tiled=True).astype(jnp.float32),
    )
    own_rows = query.shape[0]
    total_in = lax.dynamic_slice_in_dim(total_all, lax.axis_index("kv") * own_rows, own_rows, 0)
    factor = lax.rsqrt(total_in / D + EPS)[:, None]
    query, keys, values, gates = (query * factor, keys * factor, values * factor, gates * factor)
    local_rows = query.shape[0]
    heads_dev = H // lax.axis_size("tp")
    turned_query = rotate(query.reshape(local_rows, heads_dev, DK), seq_pos)
    turned_keys = rotate(keys.reshape(local_rows, heads_dev, DK), seq_pos) * DK ** (-0.5)
    head_ids = (lax.axis_index("tp") * heads_dev + jnp.arange(heads_dev, dtype=jnp.int32)).astype(
        jnp.float32
    )
    decay = head_decay(head_ids)
    new_state = decay[None, :, None, None] * state + jnp.einsum(
        "bhk,bhv->bhkv",
        turned_keys,
        values.reshape(local_rows, heads_dev, DV),
        precision=lax.Precision.HIGHEST,
    )
    read = jnp.einsum("bhk,bhkv->bhv", turned_query, new_state, precision=lax.Precision.HIGHEST)
    read = read * lax.rsqrt(jnp.mean(read * read, axis=-1, keepdims=True) + EPS)
    mixed = (
        read.reshape(local_rows, heads_dev * DV) * head_gain[None, :] * jax.nn.silu(gates)
    ).astype(jnp.bfloat16)
    attn_terms = jnp.dot(
        lax.all_gather(mixed, "kv", axis=0, tiled=True),
        out_weight,
        preferred_element_type=jnp.float32,
    )
    attn = lax.psum_scatter(
        attn_terms.astype(jnp.bfloat16), "tp", scatter_dimension=0, tiled=True
    ).astype(jnp.float32)
    resid = (tokens.astype(jnp.float32) + attn).astype(jnp.bfloat16)
    resid_all = lax.all_gather(resid, "tp", axis=0, tiled=True)
    resid_f = resid_all.astype(jnp.float32)
    squares_mid = jnp.sum(resid_f * resid_f, axis=1)
    normed_mid = (resid_f * norm_mlp_gain[None, :]).astype(jnp.bfloat16)
    term_hidden = jnp.dot(normed_mid, hidden_weight, preferred_element_type=jnp.float32).astype(
        jnp.bfloat16
    )
    total_mid = lax.psum(squares_mid, "kv")
    scale_mid = lax.rsqrt(total_mid / D + EPS)[:, None]
    hidden = lax.psum(term_hidden, "kv").astype(jnp.float32)
    active = jnp.square(jax.nn.relu(hidden * scale_mid)).astype(jnp.bfloat16)
    down_terms = jnp.dot(active, down_weight, preferred_element_type=jnp.float32)
    down = lax.psum_scatter(
        down_terms.astype(jnp.bfloat16), "tp", scatter_dimension=0, tiled=True
    ).astype(jnp.float32)
    output = (resid.astype(jnp.float32) + down).astype(jnp.bfloat16)
    return (output, new_state)


def solution(mesh):
    placed = (
        P("tp", "kv"),
        P("kv"),
        P("kv", "tp", None, None),
        P("kv"),
        P("kv", "tp"),
        P("kv", "tp"),
        P("kv", "tp"),
        P("kv", "tp"),
        P("tp"),
        P("tp", "kv"),
        P("kv"),
        P("kv", "tp"),
        P("tp", "kv"),
    )
    return jax.shard_map(
        local,
        mesh=mesh,
        in_specs=placed,
        out_specs=(P("tp", "kv"), P("kv", "tp", None, None)),
        check_vma=False,
    )
```

profile of v0, /device:TPU:0, one launch (start us, length us, event | category | flops | bytes accessed | tf_op | source)
XLA Modules:
  0.0 445.5 jit_solution(3664040884219889815)
XLA Ops:
  7.2 6.9 %all_gather.9 = bf16[128,512]{1,0:T(8,128)(2,1)S(1)} all-gather(bf16[32,512]{1,0:T(8,128)(2,1)} %param.13), channel_id=1, replica_groups=mesh['kv'=8,'tp'=4] {'tp'}, dimensions={0}, use_global_device_ids=true | all-gather | bytes 163840 | tf_op jit(solution)/shard_map/all_gather | solution.py:44
  14.1 2.0 convolution_convert_fusion.4
  16.1 1.9 convolution_convert_fusion.5
  18.1 1.7 convolution_convert_fusion.2
  19.9 2.2 convolution_convert_fusion.1
  22.4 22.1 %psum.21 = f32[128]{0:T(128)S(1)} all-reduce(f32[128]{0:T(128)S(1)} %fusion.3), channel_id=1, replica_groups=mesh['kv'=8,'tp'=4] {'kv'}, use_global_device_ids=true, to_apply=%region_2.0 | all-reduce | flops 128 | bytes 1024 | tf_op jit(solution)/shard_map/psum | solution.py:60
  44.7 35.0 %reduce-scatter.9.cloned.1.call-done = bf16[16,512]{1,0:T(8,128)(2,1)} async-done(((bf16[128,512]{1,0:T(8,128)(2,1)}), bf16[16,512]{1,0:T(8,128)(2,1)}) %reduce-scatter.9.cloned.1.call-update) | async-done | bytes 16400 | tf_op jit(solution)/shard_map/reduce_scatter | solution.py:63
  79.7 64.2 %reduce-scatter.7.cloned.1.call-done = bf16[16,512]{1,0:T(8,128)(2,1)} async-done(((bf16[128,512]{1,0:T(8,128)(2,1)}), bf16[16,512]{1,0:T(8,128)(2,1)}) %reduce-scatter.7.cloned.1.call-update) | async-done | bytes 16400 | tf_op jit(solution)/shard_map/reduce_scatter | solution.py:62
  144.9 64.0 %reduce-scatter.11.cloned.1.call-done = bf16[16,1024]{1,0:T(8,128)(2,1)} async-done(((bf16[128,1024]{1,0:T(8,128)(2,1)}), bf16[16,1024]{1,0:T(8,128)(2,1)}) %reduce-scatter.11.cloned.1.call-update) | async-done | bytes 32784 | tf_op jit(solution)/shard_map/reduce_scatter | solution.py:64
  208.9 0.8 convert_multiply_fusion.4
  209.7 4.1 multiply_add_fusion
  213.9 4.1 fusion.14
  218.3 55.3 %reduce-scatter.13.cloned.1.call-done = bf16[16,1024]{1,0:T(8,128)(2,1)} async-done(((bf16[128,1024]{1,0:T(8,128)(2,1)}), bf16[16,1024]{1,0:T(8,128)(2,1)}) %reduce-scatter.13.cloned.1.call-update) | async-done | bytes 32784 | tf_op jit(solution)/shard_map/reduce_scatter | solution.py:65
  273.6 0.9 multiply_convert_fusion.2
  274.4 30.9 %all_gather.10 = bf16[128,1024]{1,0:T(8,128)(2,1)S(1)} all-gather(bf16[16,1024]{1,0:T(8,128)(2,1)S(1)} %multiply_convert_fusion.2), channel_id=1, replica_groups=mesh['kv'=8,'tp'=4] {'kv'}, dimensions={0}, use_global_device_ids=true | all-gather | bytes 294912 | tf_op jit(solution)/shard_map/all_gather | solution.py:91
  305.3 1.0 convolution_convert_fusion.6
  306.4 18.8 %reduce-scatter.15.cloned.1.call-done = bf16[32,512]{1,0:T(8,128)(2,1)} async-done(((bf16[128,512]{1,0:T(8,128)(2,1)}), bf16[32,512]{1,0:T(8,128)(2,1)}) %reduce-scatter.15.cloned.1.call-update) | async-done | bytes 32784 | tf_op jit(solution)/shard_map/reduce_scatter | solution.py:95
  325.9 5.4 %all_gather.11 = bf16[128,512]{1,0:T(8,128)(2,1)S(1)} all-gather(bf16[32,512]{1,0:T(8,128)(2,1)S(1)} %add_convert_fusion.1), channel_id=1, replica_groups=mesh['kv'=8,'tp'=4] {'tp'}, dimensions={0}, use_global_device_ids=true | all-gather | bytes 163840 | tf_op jit(solution)/shard_map/all_gather | solution.py:99
  331.3 3.9 convolution_convert_fusion
  335.5 21.6 %psum.23 = f32[128]{0:T(128)S(1)} all-reduce(f32[128]{0:T(128)S(1)} %fusion.5), channel_id=1, replica_groups=mesh['kv'=8,'tp'=4] {'kv'}, use_global_device_ids=true, to_apply=%region_10.11 | all-reduce | flops 128 | bytes 1024 | tf_op jit(solution)/shard_map/psum | solution.py:106
  357.1 56.9 %all-reduce.2.cloned.1.call-done = bf16[128,4096]{1,0:T(8,128)(2,1)} async-done(((bf16[128,4096]{1,0:T(8,128)(2,1)}), bf16[128,4096]{1,0:T(8,128)(2,1)}) %all-reduce.2.cloned.1.call-update) | async-done | bytes 1048592 | tf_op jit(solution)/shard_map/psum | solution.py:108
  414.0 3.9 convolution_convert_fusion.3
  417.9 19.4 %reduce-scatter.17.cloned.1.call-done = bf16[32,512]{1,0:T(8,128)(2,1)} async-done(((bf16[128,512]{1,0:T(8,128)(2,1)}), bf16[32,512]{1,0:T(8,128)(2,1)}) %reduce-scatter.17.cloned.1.call-update) | async-done | bytes 32784 | tf_op jit(solution)/shard_map/reduce_scatter | solution.py:111
  437.3 1.4 add_convert_fusion
  (47 shorter events, 2.9 us)
Async XLA Ops:
  7.2 11.0 %copy-start = (bf16[512,1024]{1,0:T(8,128)(2,1)S(1)}, bf16[512,1024]{1,0:T(8,128)(2,1)}, u32[]{:S(2)}) copy-start(bf16[512,1024]{1,0:T(8,128)(2,1)} %param.19) | copy-start | bytes 3145732
  7.2 15.2 %copy-start.6 = (s32[16]{0:T(128)S(1)}, s32[16]{0:T(128)}, u32[]{:S(2)}) copy-start(s32[16]{0:T(128)} %param.14) | copy-start | bytes 196
  7.2 72.5 %reduce-scatter.9.cloned.1.call-start = ((), (), s32[]{:S(2)}) async-start(), calls=%async_computation.7 | async-start | bytes 147456 | tf_op jit(solution)/shard_map/reduce_scatter | solution.py:63
  16.1 127.8 %reduce-scatter.7.cloned.1.call-start = ((), (), s32[]{:S(2)}) async-start(), calls=%async_computation.6 | async-start | bytes 147456 | tf_op jit(solution)/shard_map/reduce_scatter | solution.py:62
  18.1 190.8 %reduce-scatter.11.cloned.1.call-start = ((), (), s32[]{:S(2)}) async-start(), calls=%async_computation.8 | async-start | bytes 294912 | tf_op jit(solution)/shard_map/reduce_scatter | solution.py:64
  19.9 253.7 %reduce-scatter.13.cloned.1.call-start = ((), (), s32[]{:S(2)}) async-start(), calls=%async_computation.9 | async-start | bytes 294912 | tf_op jit(solution)/shard_map/reduce_scatter | solution.py:65
  22.2 303.0 %reduce-scatter.15.cloned.1.call-start = ((), (), s32[]{:S(2)}) async-start(), calls=%async_computation.10 | async-start | bytes 163840 | tf_op jit(solution)/shard_map/reduce_scatter | solution.py:95
  213.9 4.1 copy-start.1
  213.9 59.7 %copy-start.4 = (f32[1024]{0:T(1024)S(1)}, f32[1024]{0:T(1024)}, u32[]{:S(2)}) copy-start(f32[1024]{0:T(1024)} %param.21) | copy-start | bytes 12292
  213.9 91.4 %copy-start.2 = (bf16[1024,512]{1,0:T(8,128)(2,1)S(1)}, bf16[1024,512]{1,0:T(8,128)(2,1)}, u32[]{:S(2)}) copy-start(bf16[1024,512]{1,0:T(8,128)(2,1)} %param.22) | copy-start | bytes 3145732
  213.9 111.2 %copy-start.3 = (bf16[32,512]{1,0:T(8,128)(2,1)S(1)}, bf16[32,512]{1,0:T(8,128)(2,1)}, u32[]{:S(2)}) copy-start(bf16[32,512]{1,0:T(8,128)(2,1)} %param.13) | copy-start | bytes 98308
  213.9 117.4 %copy-start.5 = (f32[512]{0:T(512)S(1)}, f32[512]{0:T(512)}, u32[]{:S(2)}) copy-start(f32[512]{0:T(512)} %param.23) | copy-start | bytes 6148
  306.3 107.6 %all-reduce.2.cloned.1.call-start = ((), (), s32[]{:S(2)}) async-start(), calls=%async_computation.11 | async-start | bytes 2097152 | tf_op jit(solution)/shard_map/psum | solution.py:108
  335.3 102.0 %reduce-scatter.17.cloned.1.call-start = ((), (), s32[]{:S(2)}) async-start(), calls=%async_computation.12 | async-start | bytes 163840 | tf_op jit(solution)/shard_map/reduce_scatter | solution.py:111
Sparse Core Ops, SparseCore 0:
  16.2 63.4 reduce-scatter.8
  83.0 60.8 reduce-scatter.6
  147.8 61.0 reduce-scatter.10
  212.1 61.4 reduce-scatter.12
  306.5 18.6 reduce-scatter.14
  335.4 78.4 all-reduce.1
  418.0 19.2 reduce-scatter.16
where the time goes:
time: 446 us
  waiting for transfers between devices  314 us (70%)
  blocking collectives  86.9 us (19%)
  matrix products  20.8 us (5%)
  between operations  14.3 us (3%)
  other arithmetic  9.62 us (2%)
    reduce_scatter x1, waiting for transfers between devices, local(): lax.psum_scatter(term_query, 'kv', scatter_dimension=0, tiled=True)  64.2 us
    reduce_scatter x1, waiting for transfers between devices, local(): lax.psum_scatter(term_values, 'kv', scatter_dimension=0, tiled=True)  64 us
    psum x1, waiting for transfers between devices, local(): hidden = lax.psum(term_hidden, 'kv').astype(jnp.float32)  56.9 us
    reduce_scatter x1, waiting for transfers between devices, local(): lax.psum_scatter(term_gates, 'kv', scatter_dimension=0, tiled=True)  55.3 us
    reduce_scatter x1, waiting for transfers between devices, local(): lax.psum_scatter(term_keys, 'kv', scatter_dimension=0, tiled=True)  35 us
    all_gather x1, blocking collectives, local(): lax.all_gather(mixed, 'kv', axis=0, tiled=True)  30.9 us
    psum x1, blocking collectives, local(): total_all = lax.psum(squares_in, 'kv')  22.1 us
    psum x1, blocking collectives, local(): total_mid = lax.psum(squares_mid, 'kv')  21.6 us
  transfers between devices with their start and end apart: 7, of which 7 were waited for; matrix products, arithmetic and copies ran while one was open for 4% of the time, Pallas kernels for 0%

commit v1 on v0

--- a/solution.py
+++ b/solution.py
@@ -105,7 +105,7 @@
     )
     total_mid = lax.psum(squares_mid, "kv")
     scale_mid = lax.rsqrt(total_mid / D + EPS)[:, None]
-    hidden = lax.psum(term_hidden, "kv").astype(jnp.float32)
+    hidden = lax.all_gather(term_hidden, "kv").sum(axis=0).astype(jnp.float32)
     active = jnp.square(jax.nn.relu(hidden * scale_mid)).astype(jnp.bfloat16)
     down_terms = jnp.dot(active, down_weight, preferred_element_type=jnp.float32)
     down = lax.psum_scatter(

time: 446 us -> 496 us (1.11)
  waiting for transfers between devices: 314 us -> 358 us
    all_gather x0 -> x1, waiting for transfers between devices: none -> 103 us  [local(): hidden = lax.all_gather(term_hidden, 'kv').sum(axis=0).astype(jnp.float32)]
    psum x1 -> x0, waiting for transfers between devices: 56.9 us -> none  [local(): hidden = lax.psum(term_hidden, 'kv').astype(jnp.float32)]
  transfers between devices with their start and end apart: 7 -> 7, of which waited for: 7 -> 7; matrix products, arithmetic and copies ran while one was open for 4% -> 3% of each run, Pallas kernels for 0% -> 0%
where the time goes in v1:
time: 496 us; the launch traced here: 495 us
  waiting for transfers between devices  358 us (72%)
  blocking collectives  87.2 us (18%)
  matrix products  20.5 us (4%)
  other arithmetic  14.5 us (3%)
  between operations  14.3 us (3%)
    all_gather x1, waiting for transfers between devices, local(): hidden = lax.all_gather(term_hidden, 'kv').sum(axis=0).astype(jnp.float32)  103 us
    reduce_scatter x1, waiting for transfers between devices, local(): lax.psum_scatter(term_query, 'kv', scatter_dimension=0, tiled=True)  64.2 us
    reduce_scatter x1, waiting for transfers between devices, local(): lax.psum_scatter(term_values, 'kv', scatter_dimension=0, tiled=True)  64 us
    reduce_scatter x1, waiting for transfers between devices, local(): lax.psum_scatter(term_gates, 'kv', scatter_dimension=0, tiled=True)  55.3 us
    reduce_scatter x1, waiting for transfers between devices, local(): lax.psum_scatter(term_keys, 'kv', scatter_dimension=0, tiled=True)  35 us
    all_gather x1, blocking collectives, local(): lax.all_gather(mixed, 'kv', axis=0, tiled=True)  30.9 us
    psum x1, blocking collectives, local(): total_all = lax.psum(squares_in, 'kv')  22.1 us
    psum x1, blocking collectives, local(): total_mid = lax.psum(squares_mid, 'kv')  21.9 us
  transfers between devices with their start and end apart: 7, of which 7 were waited for; matrix products, arithmetic and copies ran while one was open for 3% of the time, Pallas kernels for 0%

profile of v1, /device:TPU:0, one launch (start us, length us, event | category | flops | bytes accessed | tf_op | source)
XLA Modules:
  0.0 494.9 jit_solution(8923346000337683022)
XLA Ops:
  7.2 6.9 %all_gather.15 = bf16[128,512]{1,0:T(8,128)(2,1)S(1)} all-gather(bf16[32,512]{1,0:T(8,128)(2,1)} %param.13), channel_id=1, replica_groups=mesh['kv'=8,'tp'=4] {'tp'}, dimensions={0}, use_global_device_ids=true | all-gather | bytes 163840 | tf_op jit(solution)/shard_map/all_gather | solution.py:44
  14.1 2.0 convolution_convert_fusion.4
  16.1 1.9 convolution_convert_fusion.5
  18.1 1.7 convolution_convert_fusion.2
  19.9 2.2 convolution_convert_fusion.1
  22.4 22.1 %psum.14 = f32[128]{0:T(128)S(1)} all-reduce(f32[128]{0:T(128)S(1)} %fusion.3), channel_id=1, replica_groups=mesh['kv'=8,'tp'=4] {'kv'}, use_global_device_ids=true, to_apply=%region_2.0 | all-reduce | flops 128 | bytes 1024 | tf_op jit(solution)/shard_map/psum | solution.py:60
  44.7 35.0 %reduce-scatter.9.cloned.1.call-done = bf16[16,512]{1,0:T(8,128)(2,1)} async-done(((bf16[128,512]{1,0:T(8,128)(2,1)}), bf16[16,512]{1,0:T(8,128)(2,1)}) %reduce-scatter.9.cloned.1.call-update) | async-done | bytes 16400 | tf_op jit(solution)/shard_map/reduce_scatter | solution.py:63
  79.7 64.2 %reduce-scatter.7.cloned.1.call-done = bf16[16,512]{1,0:T(8,128)(2,1)} async-done(((bf16[128,512]{1,0:T(8,128)(2,1)}), bf16[16,512]{1,0:T(8,128)(2,1)}) %reduce-scatter.7.cloned.1.call-update) | async-done | bytes 16400 | tf_op jit(solution)/shard_map/reduce_scatter | solution.py:62
  144.9 64.0 %reduce-scatter.11.cloned.1.call-done = bf16[16,1024]{1,0:T(8,128)(2,1)} async-done(((bf16[128,1024]{1,0:T(8,128)(2,1)}), bf16[16,1024]{1,0:T(8,128)(2,1)}) %reduce-scatter.11.cloned.1.call-update) | async-done | bytes 32784 | tf_op jit(solution)/shard_map/reduce_scatter | solution.py:64
  209.7 4.1 multiply_add_fusion
  213.9 4.1 fusion.14
  218.3 55.3 %reduce-scatter.13.cloned.1.call-done = bf16[16,1024]{1,0:T(8,128)(2,1)} async-done(((bf16[128,1024]{1,0:T(8,128)(2,1)}), bf16[16,1024]{1,0:T(8,128)(2,1)}) %reduce-scatter.13.cloned.1.call-update) | async-done | bytes 32784 | tf_op jit(solution)/shard_map/reduce_scatter | solution.py:65
  273.6 0.9 multiply_convert_fusion.2
  274.4 30.9 %all_gather.16 = bf16[128,1024]{1,0:T(8,128)(2,1)S(1)} all-gather(bf16[16,1024]{1,0:T(8,128)(2,1)S(1)} %multiply_convert_fusion.2), channel_id=1, replica_groups=mesh['kv'=8,'tp'=4] {'kv'}, dimensions={0}, use_global_device_ids=true | all-gather | bytes 294912 | tf_op jit(solution)/shard_map/all_gather | solution.py:91
  305.3 1.0 convolution_convert_fusion.6
  306.4 18.8 %reduce-scatter.15.cloned.1.call-done = bf16[32,512]{1,0:T(8,128)(2,1)} async-done(((bf16[128,512]{1,0:T(8,128)(2,1)}), bf16[32,512]{1,0:T(8,128)(2,1)}) %reduce-scatter.15.cloned.1.call-update) | async-done | bytes 32784 | tf_op jit(solution)/shard_map/reduce_scatter | solution.py:95
  325.9 5.4 %all_gather.17 = bf16[128,512]{1,0:T(8,128)(2,1)S(1)} all-gather(bf16[32,512]{1,0:T(8,128)(2,1)S(1)} %add_convert_fusion.1), channel_id=1, replica_groups=mesh['kv'=8,'tp'=4] {'tp'}, dimensions={0}, use_global_device_ids=true | all-gather | bytes 163840 | tf_op jit(solution)/shard_map/all_gather | solution.py:99
  331.3 4.0 convolution_convert_fusion
  335.5 21.9 %psum.15 = f32[128]{0:T(128)S(1)} all-reduce(f32[128]{0:T(128)S(1)} %fusion.5), channel_id=1, replica_groups=mesh['kv'=8,'tp'=4] {'kv'}, use_global_device_ids=true, to_apply=%region_10.11 | all-reduce | flops 128 | bytes 1024 | tf_op jit(solution)/shard_map/psum | solution.py:106
  357.5 102.6 %all-gather.3.cloned.1.call-done = bf16[1024,4096]{1,0:T(8,128)(2,1)} async-done(((bf16[128,4096]{1,0:T(8,128)(2,1)}), bf16[1024,4096]{1,0:T(8,128)(2,1)}) %all-gather.3.cloned.1.call-update) | async-done | bytes 8388624 | tf_op jit(solution)/shard_map/all_gather | solution.py:108
  460.1 4.9 reduce_sum.41
  465.0 3.6 convolution_convert_fusion.3
  468.6 18.0 %reduce-scatter.17.cloned.1.call-done = bf16[32,512]{1,0:T(8,128)(2,1)} async-done(((bf16[128,512]{1,0:T(8,128)(2,1)}), bf16[32,512]{1,0:T(8,128)(2,1)}) %reduce-scatter.17.cloned.1.call-update) | async-done | bytes 32784 | tf_op jit(solution)/shard_map/reduce_scatter | solution.py:111
  486.6 1.4 add_convert_fusion
  (48 shorter events, 3.8 us)
Async XLA Ops:
  7.2 11.0 %copy-start = (bf16[512,1024]{1,0:T(8,128)(2,1)S(1)}, bf16[512,1024]{1,0:T(8,128)(2,1)}, u32[]{:S(2)}) copy-start(bf16[512,1024]{1,0:T(8,128)(2,1)} %param.19) | copy-start | bytes 3145732
  7.2 15.2 %copy-start.6 = (s32[16]{0:T(128)S(1)}, s32[16]{0:T(128)}, u32[]{:S(2)}) copy-start(s32[16]{0:T(128)} %param.14) | copy-start | bytes 196
  7.2 72.5 %reduce-scatter.9.cloned.1.call-start = ((), (), s32[]{:S(2)}) async-start(), calls=%async_computation.7 | async-start | bytes 147456 | tf_op jit(solution)/shard_map/reduce_scatter | solution.py:63
  16.1 127.8 %reduce-scatter.7.cloned.1.call-start = ((), (), s32[]{:S(2)}) async-start(), calls=%async_computation.6 | async-start | bytes 147456 | tf_op jit(solution)/shard_map/reduce_scatter | solution.py:62
  18.1 190.8 %reduce-scatter.11.cloned.1.call-start = ((), (), s32[]{:S(2)}) async-start(), calls=%async_computation.8 | async-start | bytes 294912 | tf_op jit(solution)/shard_map/reduce_scatter | solution.py:64
  19.9 253.7 %reduce-scatter.13.cloned.1.call-start = ((), (), s32[]{:S(2)}) async-start(), calls=%async_computation.9 | async-start | bytes 294912 | tf_op jit(solution)/shard_map/reduce_scatter | solution.py:65
  22.2 303.0 %reduce-scatter.15.cloned.1.call-start = ((), (), s32[]{:S(2)}) async-start(), calls=%async_computation.10 | async-start | bytes 163840 | tf_op jit(solution)/shard_map/reduce_scatter | solution.py:95
  213.9 4.1 copy-start.1
  213.9 59.7 %copy-start.4 = (f32[1024]{0:T(1024)S(1)}, f32[1024]{0:T(1024)}, u32[]{:S(2)}) copy-start(f32[1024]{0:T(1024)} %param.21) | copy-start | bytes 12292
  213.9 91.4 %copy-start.2 = (bf16[1024,512]{1,0:T(8,128)(2,1)S(1)}, bf16[1024,512]{1,0:T(8,128)(2,1)}, u32[]{:S(2)}) copy-start(bf16[1024,512]{1,0:T(8,128)(2,1)} %param.22) | copy-start | bytes 3145732
  213.9 111.2 %copy-start.3 = (bf16[32,512]{1,0:T(8,128)(2,1)S(1)}, bf16[32,512]{1,0:T(8,128)(2,1)}, u32[]{:S(2)}) copy-start(bf16[32,512]{1,0:T(8,128)(2,1)} %param.13) | copy-start | bytes 98308
  213.9 117.4 %copy-start.5 = (f32[512]{0:T(512)S(1)}, f32[512]{0:T(512)}, u32[]{:S(2)}) copy-start(f32[512]{0:T(512)} %param.23) | copy-start | bytes 6148
  306.3 153.8 %all-gather.3.cloned.1.call-start = ((), (), s32[]{:S(2)}) async-start(), calls=%async_computation.12 | async-start | bytes 9437184 | tf_op jit(solution)/shard_map/all_gather | solution.py:108
  335.4 151.3 %reduce-scatter.17.cloned.1.call-start = ((), (), s32[]{:S(2)}) async-start(), calls=%async_computation.11 | async-start | bytes 163840 | tf_op jit(solution)/shard_map/reduce_scatter | solution.py:111
Sparse Core Ops, SparseCore 0:
  16.2 63.4 reduce-scatter.8
  83.0 60.8 reduce-scatter.6
  147.8 61.0 reduce-scatter.10
  212.1 61.4 reduce-scatter.12
  306.5 18.6 reduce-scatter.14
  335.5 124.5 all-gather.2
  468.8 17.8 reduce-scatter.16
